TPU v7x, 32 devices: a whole 2x2x4 slice. The times are simulated.
32 devices in a mesh: fs: 8 (over z, y), tp: 4 (over x, core).
Axes of the slice: x: 2, y: 2, z: 4, core: 2. Of those that a mesh axis runs over, the one named last changes fastest.
Arguments:
- mixed: bfloat16 [12288, 2048], P(('fs', 'tp')), may hold values from -6 to 6
- residual: bfloat16 [12288, 2048], P(('fs', 'tp')), may hold values from -6 to 6
- mix_weight: bfloat16 [2048, 2048], P(('fs', 'tp')), may hold values from -0.125 to 0.125
- norm_gain: float32 [2048], replicated, may hold values from 0.1 to 1.9
- up_weight: bfloat16 [2048, 5504], P('fs', 'tp'), may hold values from -0.125 to 0.125
- gate_weight: bfloat16 [2048, 5504], P('fs', 'tp'), may hold values from -0.125 to 0.125
- conv_weight: float32 [3, 5504], P(None, 'tp'), may hold values from -3 to 3
- conv_bias: float32 [5504], P('tp'), may hold values from -3 to 3
- down_weight: bfloat16 [5504, 2048], P('tp', 'fs'), may hold values from -0.078125 to 0.078125
Outputs:
- output: bfloat16 [12288, 2048], P(('fs', 'tp'))
All inputs are finite; a program needn't handle non-finite values.
Results may differ from a plain program's by a relative error of at most 0.012.
Values may be sent and summed in bfloat16 or wider, within the bound.
A program may use at most 128 MiB of HBM per device.

v0:
```python
import jax
import jax.numpy as jnp
from jax import lax
from jax.sharding import PartitionSpec as P

norm_eps = 1e-06


def body(
    mixed,
    residual,
    mix_weight,
    norm_gain,
    up_weight,
    gate_weight,
    conv_weight,
    conv_bias,
    down_weight,
):
    summed = jnp.dot(
        mixed,
        lax.all_gather(mix_weight, ("fs", "tp"), axis=0, tiled=True),
        preferred_element_type=jnp.float32,
    )
    stream = (residual.astype(jnp.float32) + summed).astype(jnp.bfloat16)
    x_float = stream.astype(jnp.float32)
    normed = (
        x_float
        * lax.rsqrt(jnp.mean(x_float * x_float, axis=-1, keepdims=True) + norm_eps)
        * norm_gain
    ).astype(jnp.bfloat16)
    half_cols = up_weight.shape[1]
    up_full, gate_full = (
        lax.all_gather(up_weight, "fs", axis=0, tiled=True),
        lax.all_gather(gate_weight, "fs", axis=0, tiled=True),
    )
    shard_piece = lax.all_gather(normed, "tp", axis=0, tiled=True)
    up_rows = jnp.dot(shard_piece, up_full, preferred_element_type=jnp.float32).astype(jnp.bfloat16)
    gate_rows = jnp.dot(shard_piece, gate_full, preferred_element_type=jnp.float32).astype(
        jnp.bfloat16
    )
    joined = jnp.concatenate([up_rows, gate_rows], axis=1)
    up_part = joined[:, :half_cols]
    gate_part = joined[:, half_cols:]
    up_float = lax.optimization_barrier(up_part).astype(jnp.float32)
    padded = jnp.pad(up_float, ((2, 0), (0, 0)))
    smoothed = (
        conv_bias
        + conv_weight[0] * padded[:-2]
        + conv_weight[1] * padded[1:-1]
        + conv_weight[2] * padded[2:]
    )
    hidden = (jax.nn.gelu(smoothed) * gate_part.astype(jnp.float32)).astype(jnp.bfloat16)
    down_full = lax.all_gather(down_weight, "fs", axis=1, tiled=True)
    summed_out = lax.psum_scatter(
        jnp.dot(hidden, down_full, preferred_element_type=jnp.float32).astype(jnp.bfloat16),
        "tp",
        scatter_dimension=0,
        tiled=True,
    ).astype(jnp.float32)
    return (x_float + summed_out).astype(jnp.bfloat16)


def solution(mesh):
    return jax.shard_map(
        body,
        mesh=mesh,
        in_specs=(
            P(("fs", "tp"), None),
            P(("fs", "tp"), None),
            P(("fs", "tp"), None),
            P(),
            P("fs", "tp"),
            P("fs", "tp"),
            P(None, "tp"),
            P("tp"),
            P("tp", "fs"),
        ),
        out_specs=P(("fs", "tp"), None),
        check_vma=False,
    )
```

profile of v0, /device:TPU:0, one launch (start us, length us, event | category | flops | bytes accessed | tf_op | source)
XLA Modules:
  0.0 495.7 jit_solution(2347268354048013400)
XLA Ops:
  6.5 0.0 copy-start
  6.5 0.0 all-gather.6.cloned.1.call-start
  6.5 0.7 all-gather.6.cloned.1.call-update
  7.3 0.0 all-gather.10.cloned.1.call-start
  7.3 0.7 all-gather.10.cloned.1.call-update
  8.0 0.0 copy-start.2
  8.0 0.0 all-gather.8.cloned.1.call-start
  8.1 81.9 %all-gather.6.cloned.1.call-done = bf16[2048,2048]{1,0:T(8,128)(2,1)} async-done(((bf16[64,2048]{1,0:T(8,128)(2,1)}), bf16[2048,2048]{1,0:T(8,128)(2,1)}) %all-gather.6.cloned.1.call-update) | async-done | bytes 8388624 | tf_op jit(solution)/shard_map/all_gather | solution.py:22
  90.0 0.0 copy-done
  90.0 7.4 %fusion.22 = (f32[384]{0:T(512)S(1)}, bf16[384,2048]{1,0:T(8,128)(2,1)S(1)}) fusion(bf16[384,2048]{1,0:T(8,128)(2,1)S(1)} %copy-done, bf16[2048,2048]{1,0:T(8,128)(2,1)} %all-gather.6.cloned.1.call-done, bf16[384,2048]{1,0:T(8,128)(2,1)} %param.10), kind=kOutput, calls=%fused_computation.31 | convolution fusion | flops 3225943552 | bytes 13108736 | tf_op jit(solution)/shard_map/dot_general | solution.py:20
  97.4 0.0 copy-start.1
  97.4 0.0 copy-done.2
  97.4 1.6 fusion.24
  99.0 0.0 all-gather.8.cloned.1.call-update
  99.0 0.0 all-gather.12.cloned.1.call-start
  99.0 0.5 all-gather.12.cloned.1.call-update
  99.6 0.0 all-gather.14.cloned.1.call-start
  99.6 0.5 all-gather.14.cloned.1.call-update
  100.2 0.2 reduce-scatter.2.cloned.1.call-start
  100.4 0.0 copy-done.1
  100.4 0.1 slice_reduce_fusion.2
  100.5 81.8 %all-gather.10.cloned.1.call-done = bf16[2048,1376]{0,1:T(8,128)(2,1)} async-done(((bf16[256,1376]{0,1:T(8,128)(2,1)}), bf16[2048,1376]{0,1:T(8,128)(2,1)}) %all-gather.10.cloned.1.call-update) | async-done | bytes 5636112 | tf_op jit(solution)/shard_map/all_gather | solution.py:34
  182.2 46.1 %all-gather.8.cloned.1.call-done = bf16[1536,2048]{1,0:T(8,128)(2,1)} async-done(((bf16[384,2048]{1,0:T(8,128)(2,1)}), bf16[1536,2048]{1,0:T(8,128)(2,1)}) %all-gather.8.cloned.1.call-update) | async-done | bytes 6291472 | tf_op jit(solution)/shard_map/all_gather | solution.py:37
  228.4 12.8 %convolution_convert_fusion.2 = bf16[1536,1376]{0,1:T(8,128)(2,1)S(1)} fusion(bf16[1536,2048]{1,0:T(8,128)(2,1)} %all-gather.8.cloned.1.call-done, bf16[2048,1376]{0,1:T(8,128)(2,1)} %all-gather.10.cloned.1.call-done), kind=kOutput, calls=%fused_computation.19 | convolution fusion | flops 8659156992 | bytes 16154624 | tf_op jit(solution)/shard_map/dot_general | solution.py:38
  241.2 0.0 copy-start.3
  241.2 4.5 convert_element_type.43
  245.7 76.1 %all-gather.12.cloned.1.call-done = bf16[2048,1376]{0,1:T(8,128)(2,1)} async-done(((bf16[256,1376]{0,1:T(8,128)(2,1)}), bf16[2048,1376]{0,1:T(8,128)(2,1)}) %all-gather.12.cloned.1.call-update) | async-done | bytes 5636112 | tf_op jit(solution)/shard_map/all_gather | solution.py:35
  321.9 0.0 copy-done.3
  321.9 21.8 %fusion.13.clone.4 = bf16[1536,1376]{0,1:T(8,128)(2,1)} fusion(f32[1536,1376]{0,1:T(8,128)} %convert_element_type.43, bf16[1536,2048]{1,0:T(8,128)(2,1)} %all-gather.8.cloned.1.call-done, bf16[2048,1376]{0,1:T(8,128)(2,1)} %all-gather.12.cloned.1.call-done, f32[1376]{0:T(1024)S(1)} %get-tuple-element.6, f32[1376]{0:T(1024)S(1)} %get-tuple-element.7, ...), kind=kOutput, calls=%fused_computation.16.clone.clone.clone.1 | convolution fusion | flops 8695087104 | bytes 24630784 | tf_op jit(solution)/shard_map/dot_general | solution.py:39
  343.6 69.9 %all-gather.14.cloned.1.call-done = bf16[1376,2048]{1,0:T(8,128)(2,1)} async-done(((bf16[1376,256]{1,0:T(8,128)(2,1)}), bf16[1376,2048]{1,0:T(8,128)(2,1)}) %all-gather.14.cloned.1.call-update) | async-done | bytes 5636112 | tf_op jit(solution)/shard_map/all_gather | solution.py:54
  413.5 15.0 %convolution_convert_fusion = bf16[1536,2048]{1,0:T(8,128)(2,1)} fusion(bf16[1376,2048]{1,0:T(8,128)(2,1)} %all-gather.14.cloned.1.call-done, bf16[1536,1376]{0,1:T(8,128)(2,1)} %fusion.13.clone.4), kind=kOutput, calls=%fused_computation.17 | convolution fusion | flops 8660189184 | bytes 16154624 | tf_op jit(solution)/shard_map/dot_general | solution.py:56
  428.5 0.0 reduce-scatter.2.cloned.1.call-update
  428.5 57.2 %reduce-scatter.2.cloned.1.call-done = bf16[384,2048]{1,0:T(8,128)(2,1)} async-done(((bf16[1536,2048]{1,0:T(8,128)(2,1)}), bf16[384,2048]{1,0:T(8,128)(2,1)}) %reduce-scatter.2.cloned.1.call-update) | async-done | bytes 1572880 | tf_op jit(solution)/shard_map/reduce_scatter | solution.py:55
  485.7 3.2 fusion.25
  (1 shorter events, 0.0 us)
Async XLA Ops:
  6.5 83.5 %copy-start = (bf16[384,2048]{1,0:T(8,128)(2,1)S(1)}, bf16[384,2048]{1,0:T(8,128)(2,1)}, u32[]{:S(2)}) copy-start(bf16[384,2048]{1,0:T(8,128)(2,1)} %param.9) | copy-start | bytes 4718596
  6.5 83.5 %all-gather.6.cloned.1.call-start = ((), (), s32[]{:S(2)}) async-start(), calls=%async_computation.1 | async-start | bytes 8650752 | tf_op jit(solution)/shard_map/all_gather | solution.py:22
  7.3 175.0 %all-gather.10.cloned.1.call-start = ((), (), s32[]{:S(2)}) async-start(), calls=%async_computation.3 | async-start | bytes 6340608 | tf_op jit(solution)/shard_map/all_gather | solution.py:34
  8.0 89.4 %copy-start.2 = (f32[2048]{0:T(1024)S(1)}, f32[2048]{0:T(1024)}, u32[]{:S(2)}) copy-start(f32[2048]{0:T(1024)} %param.12) | copy-start | bytes 24580
  8.0 220.4 %all-gather.8.cloned.1.call-start = ((), (), s32[]{:S(2)}) async-start(), calls=%async_computation.2 | async-start | bytes 7864320 | tf_op jit(solution)/shard_map/all_gather | solution.py:37
  97.4 3.0 copy-start.1
  99.0 222.9 %all-gather.12.cloned.1.call-start = ((), (), s32[]{:S(2)}) async-start(), calls=%async_computation.4 | async-start | bytes 6340608 | tf_op jit(solution)/shard_map/all_gather | solution.py:35
  99.6 313.9 %all-gather.14.cloned.1.call-start = ((), (), s32[]{:S(2)}) async-start(), calls=%async_computation.5 | async-start | bytes 6340608 | tf_op jit(solution)/shard_map/all_gather | solution.py:54
  100.2 385.5 %reduce-scatter.2.cloned.1.call-start = ((), (), s32[]{:S(2)}) async-start(), calls=%async_computation.6 | async-start | bytes 7864320 | tf_op jit(solution)/shard_map/reduce_scatter | solution.py:55
  241.2 80.7 %copy-start.3 = (f32[1376]{0:T(1024)S(1)}, f32[1376]{0:T(1024)}, u32[]{:S(2)}) copy-start(f32[1376]{0:T(1024)} %param.16) | copy-start | bytes 16516
Sparse Core Ops, SparseCore 0:
  10.2 79.7 all-gather.5
  92.0 90.1 all-gather.9
  183.8 44.5 all-gather.7
  230.3 91.5 all-gather.11
  323.7 89.7 all-gather.13
  428.6 57.0 reduce-scatter.1
where the time goes:
time: 496 us
  waiting for transfers between devices  416 us (84%)
  matrix products  56.9 us (11%)
  between operations  13.5 us (3%)
  other arithmetic  9.33 us (2%)
    all_gather x1, waiting for transfers between devices, body(): lax.all_gather(mix_weight, ('fs', 'tp'), axis=0, tiled=True)  81.9 us
    all_gather x1, waiting for transfers between devices, body(): lax.all_gather(up_weight, 'fs', axis=0, tiled=True)  81.8 us
    all_gather x1, waiting for transfers between devices, body(): lax.all_gather(gate_weight, 'fs', axis=0, tiled=True)  76.1 us
    all_gather x1, waiting for transfers between devices, body(): down_full = lax.all_gather(down_weight, 'fs', axis=1, tiled=True)  69.9 us
    reduce_scatter x1, waiting for transfers between devices, body(): lax.psum_scatter(jnp.dot(hidden, down_full, preferred_element_type=jnp.fl...  57.2 us
    all_gather x1, waiting for transfers between devices, body(): shard_piece = lax.all_gather(normed, 'tp', axis=0, tiled=True)  46.1 us
    dot_general x1, matrix products, body(): jnp.dot(shard_piece, gate_full, preferred_element_type=jnp.float32)  21.8 us
    dot_general x1, matrix products, body(): jnp.dot(hidden, down_full, preferred_element_type=jnp.float32)  15 us
  transfers between devices with their start and end apart: 6, of which 6 were waited for; matrix products, arithmetic and copies ran while one was open for 10% of the time, Pallas kernels for 0%

commit v1 on v0

--- a/solution.py
+++ b/solution.py
@@ -4,6 +4,16 @@
 from jax.sharding import PartitionSpec as P
 
 norm_eps = 1e-06
+
+
+def around_the_ring(array, axis, dim):
+    size = lax.axis_size(axis)
+    held, blocks = (array, [array])
+    for _ in range(size - 1):
+        held = lax.ppermute(held, axis, [(i, (i + 1) % size) for i in range(size)])
+        blocks.insert(0, held)
+    merged = jnp.concatenate(blocks, axis=dim)
+    return jnp.roll(merged, (lax.axis_index(axis) + 1) * array.shape[dim], axis=dim)
 
 
 def body(
@@ -34,7 +44,7 @@
         lax.all_gather(up_weight, "fs", axis=0, tiled=True),
         lax.all_gather(gate_weight, "fs", axis=0, tiled=True),
     )
-    shard_piece = lax.all_gather(normed, "tp", axis=0, tiled=True)
+    shard_piece = around_the_ring(normed, "tp", 0)
     up_rows = jnp.dot(shard_piece, up_full, preferred_element_type=jnp.float32).astype(jnp.bfloat16)
     gate_rows = jnp.dot(shard_piece, gate_full, preferred_element_type=jnp.float32).astype(
         jnp.bfloat16

time: 496 us -> 448 us (0.903)
  waiting for transfers between devices: 416 us -> 352 us
  local copies, waits for them, and re-layouts: 0.07 us -> 13.8 us
    all_gather x1, waiting for transfers between devices: 81.8 us -> 7.46 us  [body(): lax.all_gather(up_weight, 'fs', axis=0, tiled=True)]
    ppermute x0 -> x3, waiting for transfers between devices: none -> 59.6 us  [around_the_ring(): held = lax.ppermute(held, axis, [(i, (i + 1) % size) for i in range(size)])]
    all_gather x1 -> x0, waiting for transfers between devices: 46.1 us -> none  [body(): shard_piece = lax.all_gather(normed, 'tp', axis=0, tiled=True)]
    unnamed x8 -> x16, local copies, waits for them, and re-layouts: 0.02 us -> 13.8 us
  transfers between devices with their start and end apart: 6 -> 8, of which waited for: 6 -> 8; matrix products, arithmetic and copies ran while one was open for 10% -> 14% of each run, Pallas kernels for 0% -> 0%
where the time goes in v1:
time: 448 us
  waiting for transfers between devices  352 us (79%)
  matrix products  57.1 us (13%)
  local copies, waits for them, and re-layouts  13.8 us (3%)
  between operations  13.2 us (3%)
  other arithmetic  11.2 us (2%)
    all_gather x1, waiting for transfers between devices, body(): lax.all_gather(mix_weight, ('fs', 'tp'), axis=0, tiled=True)  81.2 us
    all_gather x1, waiting for transfers between devices, body(): lax.all_gather(gate_weight, 'fs', axis=0, tiled=True)  74.6 us
    all_gather x1, waiting for transfers between devices, body(): down_full = lax.all_gather(down_weight, 'fs', axis=1, tiled=True)  69.9 us
    ppermute x3, waiting for transfers between devices, around_the_ring(): held = lax.ppermute(held, axis, [(i, (i + 1) % size) for i in range(size)])  59.6 us
    reduce_scatter x1, waiting for transfers between devices, body(): lax.psum_scatter(jnp.dot(hidden, down_full, preferred_element_type=jnp.fl...  57.2 us
    dot_general x1, matrix products, body(): jnp.dot(shard_piece, gate_full, preferred_element_type=jnp.float32)  21.8 us
    dot_general x1, matrix products, body(): jnp.dot(hidden, down_full, preferred_element_type=jnp.float32)  15.1 us
    unnamed x16, local copies, waits for them, and re-layouts  13.8 us
  transfers between devices with their start and end apart: 8, of which 8 were waited for; matrix products, arithmetic and copies ran while one was open for 14% of the time, Pallas kernels for 0%

profile of v1, /device:TPU:0, one launch (start us, length us, event | category | flops | bytes accessed | tf_op | source)
XLA Modules:
  0.0 447.8 jit_solution(4352930181993435649)
XLA Ops:
  6.5 0.0 copy-start
  6.5 0.0 all-gather.5.cloned.1.call-start
  6.5 0.7 all-gather.5.cloned.1.call-update
  7.3 0.0 all-gather.7.cloned.1.call-start
  7.3 0.7 all-gather.7.cloned.1.call-update
  8.0 0.0 all-gather.9.cloned.1.call-start
  8.1 0.7 all-gather.9.cloned.1.call-update
  8.7 0.0 copy-start.2
  8.8 0.0 copy-start.3
  8.8 0.0 all-gather.11.cloned.1.call-start
  8.8 81.2 %all-gather.5.cloned.1.call-done = bf16[2048,2048]{1,0:T(8,128)(2,1)} async-done(((bf16[64,2048]{1,0:T(8,128)(2,1)}), bf16[2048,2048]{1,0:T(8,128)(2,1)}) %all-gather.5.cloned.1.call-update) | async-done | bytes 8388624 | tf_op jit(solution)/shard_map/all_gather | solution.py:32
  90.0 0.0 copy-done
  90.0 7.4 %fusion.25 = (f32[384]{0:T(512)S(1)}, bf16[384,2048]{1,0:T(8,128)(2,1)S(1)}) fusion(bf16[384,2048]{1,0:T(8,128)(2,1)S(1)} %copy-done, bf16[2048,2048]{1,0:T(8,128)(2,1)} %all-gather.5.cloned.1.call-done, bf16[384,2048]{1,0:T(8,128)(2,1)} %param.10), kind=kOutput, calls=%fused_computation.33 | convolution fusion | flops 3225943552 | bytes 13108736 | tf_op jit(solution)/shard_map/dot_general | solution.py:30
  97.4 0.0 copy-done.2
  97.4 0.4 fusion.27
  97.8 0.3 collective-permute-start
  98.1 19.6 %collective-permute-done = bf16[384,2048]{1,0:T(8,128)(2,1)S(1)} collective-permute-done((bf16[384,2048]{1,0:T(8,128)(2,1)S(1)}, bf16[384,2048]{1,0:T(8,128)(2,1)S(1)}, u32[]{:S(2)}, u32[]{:S(2)}) %collective-permute-start) | collective-permute-done | bytes 1572896 | tf_op jit(solution)/shard_map/ppermute | solution.py:13
  117.7 0.0 collective-permute-start.1
  117.7 0.0 all-gather.11.cloned.1.call-update
  117.7 0.0 reduce-scatter.2.cloned.1.call-start
  117.8 19.9 %collective-permute-done.1 = bf16[384,2048]{1,0:T(8,128)(2,1)} collective-permute-done((bf16[384,2048]{1,0:T(8,128)(2,1)S(1)}, bf16[384,2048]{1,0:T(8,128)(2,1)}, u32[]{:S(2)}, u32[]{:S(2)}) %collective-permute-start.1) | collective-permute-done | bytes 1572896 | tf_op jit(solution)/shard_map/ppermute | solution.py:13
  137.7 0.0 collective-permute-start.2
  137.7 0.0 copy-done.3
  137.7 20.1 %collective-permute-done.2 = bf16[384,2048]{1,0:T(8,128)(2,1)} collective-permute-done((bf16[384,2048]{1,0:T(8,128)(2,1)}, bf16[384,2048]{1,0:T(8,128)(2,1)}, u32[]{:S(2)}, u32[]{:S(2)}) %collective-permute-start.2) | collective-permute-done | bytes 1572896 | tf_op jit(solution)/shard_map/ppermute | solution.py:13
  157.8 2.7 constant_dynamic-update-slice_fusion.7
  160.6 2.7 constant_dynamic-update-slice_fusion.6
  163.3 1.3 constant_dynamic-update-slice_fusion.5
  164.6 1.6 constant_dynamic-update-slice_fusion.4
  166.2 2.8 constant_dynamic-update-slice_fusion.3
  169.0 2.8 constant_dynamic-update-slice_fusion.2
  171.9 1.3 constant_dynamic-update-slice_fusion.1
  173.2 1.6 constant_dynamic-update-slice_fusion
  174.8 7.5 %all-gather.7.cloned.1.call-done = bf16[2048,1376]{0,1:T(8,128)(2,1)} async-done(((bf16[256,1376]{0,1:T(8,128)(2,1)}), bf16[2048,1376]{0,1:T(8,128)(2,1)}) %all-gather.7.cloned.1.call-update) | async-done | bytes 5636112 | tf_op jit(solution)/shard_map/all_gather | solution.py:44
  182.2 12.8 %convolution_convert_fusion.2 = bf16[1536,1376]{0,1:T(8,128)(2,1)S(1)} fusion(bf16[2048,1376]{0,1:T(8,128)(2,1)} %all-gather.7.cloned.1.call-done, bf16[3072,2048]{1,0:T(8,128)(2,1)} %constant_dynamic-update-slice_fusion, s32[]{:T(128)S(6)} %select_n.14), kind=kOutput, calls=%fused_computation.19 | convolution fusion | flops 8659156992 | bytes 16154628 | tf_op jit(solution)/shard_map/dot_general | solution.py:48
  195.0 0.0 copy-start.4
  195.0 4.4 convert_element_type.43
  199.4 74.6 %all-gather.9.cloned.1.call-done = bf16[2048,1376]{0,1:T(8,128)(2,1)} async-done(((bf16[256,1376]{0,1:T(8,128)(2,1)}), bf16[2048,1376]{0,1:T(8,128)(2,1)}) %all-gather.9.cloned.1.call-update) | async-done | bytes 5636112 | tf_op jit(solution)/shard_map/all_gather | solution.py:45
  274.1 0.0 copy-done.4
  274.1 21.8 %fusion.13.clone.4 = bf16[1536,1376]{0,1:T(8,128)(2,1)} fusion(f32[1536,1376]{0,1:T(8,128)} %convert_element_type.43, bf16[2048,1376]{0,1:T(8,128)(2,1)} %all-gather.9.cloned.1.call-done, bf16[3072,2048]{1,0:T(8,128)(2,1)} %constant_dynamic-update-slice_fusion, s32[]{:T(128)S(6)} %select_n.14, f32[1376]{0:T(1024)S(1)} %get-tuple-element.6, ...), kind=kOutput, calls=%fused_computation.16.clone.clone.clone.1 | convolution fusion | flops 8695087104 | bytes 24630788 | tf_op jit(solution)/shard_map/dot_general | solution.py:49
  295.8 69.9 %all-gather.11.cloned.1.call-done = bf16[1376,2048]{1,0:T(8,128)(2,1)} async-done(((bf16[1376,256]{1,0:T(8,128)(2,1)}), bf16[1376,2048]{1,0:T(8,128)(2,1)}) %all-gather.11.cloned.1.call-update) | async-done | bytes 5636112 | tf_op jit(solution)/shard_map/all_gather | solution.py:64
  365.7 0.0 copy-start.1
  365.7 15.1 %convolution_convert_fusion = bf16[1536,2048]{1,0:T(8,128)(2,1)} fusion(bf16[1376,2048]{1,0:T(8,128)(2,1)} %all-gather.11.cloned.1.call-done, bf16[1536,1376]{0,1:T(8,128)(2,1)} %fusion.13.clone.4), kind=kOutput, calls=%fused_computation.17 | convolution fusion | flops 8660189184 | bytes 16154624 | tf_op jit(solution)/shard_map/dot_general | solution.py:66
  380.8 0.0 reduce-scatter.2.cloned.1.call-update
  380.9 57.2 %reduce-scatter.2.cloned.1.call-done = bf16[384,2048]{1,0:T(8,128)(2,1)} async-done(((bf16[1536,2048]{1,0:T(8,128)(2,1)}), bf16[384,2048]{1,0:T(8,128)(2,1)}) %reduce-scatter.2.cloned.1.call-update) | async-done | bytes 1572880 | tf_op jit(solution)/shard_map/reduce_scatter | solution.py:65
  438.0 3.2 fusion.28
  441.3 0.0 copy-done.1
  (2 shorter events, 0.1 us)
Async XLA Ops:
  6.5 83.5 %copy-start = (bf16[384,2048]{1,0:T(8,128)(2,1)S(1)}, bf16[384,2048]{1,0:T(8,128)(2,1)}, u32[]{:S(2)}) copy-start(bf16[384,2048]{1,0:T(8,128)(2,1)} %param.9) | copy-start | bytes 4718596
  6.5 83.5 %all-gather.5.cloned.1.call-start = ((), (), s32[]{:S(2)}) async-start(), calls=%async_computation.1 | async-start | bytes 8650752 | tf_op jit(solution)/shard_map/all_gather | solution.py:32
  7.3 175.0 %all-gather.7.cloned.1.call-start = ((), (), s32[]{:S(2)}) async-start(), calls=%async_computation.2 | async-start | bytes 6340608 | tf_op jit(solution)/shard_map/all_gather | solution.py:44
  8.0 266.0 %all-gather.9.cloned.1.call-start = ((), (), s32[]{:S(2)}) async-start(), calls=%async_computation.3 | async-start | bytes 6340608 | tf_op jit(solution)/shard_map/all_gather | solution.py:45
  8.7 88.6 %copy-start.2 = (f32[2048]{0:T(1024)S(1)}, f32[2048]{0:T(1024)}, u32[]{:S(2)}) copy-start(f32[2048]{0:T(1024)} %param.12) | copy-start | bytes 24580
  8.8 128.9 %copy-start.3 = (f32[3,1376]{1,0:T(4,128)S(1)}, f32[3,1376]{1,0:T(4,128)}, u32[]{:S(2)}) copy-start(f32[3,1376]{1,0:T(4,128)} %param.15) | copy-start | bytes 49540
  8.8 357.0 %all-gather.11.cloned.1.call-start = ((), (), s32[]{:S(2)}) async-start(), calls=%async_computation.4 | async-start | bytes 6340608 | tf_op jit(solution)/shard_map/all_gather | solution.py:64
  97.8 19.9 %collective-permute-start = (bf16[384,2048]{1,0:T(8,128)(2,1)S(1)}, bf16[384,2048]{1,0:T(8,128)(2,1)S(1)}, u32[]{:S(2)}, u32[]{:S(2)}) collective-permute-start(bf16[384,2048]{1,0:T(8,128)(2,1)S(1)} %fusion.27), channel_id=1, source_target_pairs={{0,1},{1,2},{2,3},{3,0},{4,5},{5,6},{6,7},{7,4},{8,9},{9,10},{10,1... | collective-permute-start | bytes 4718600 | tf_op jit(solution)/shard_map/ppermute | solution.py:13
  117.7 19.9 %collective-permute-start.1 = (bf16[384,2048]{1,0:T(8,128)(2,1)S(1)}, bf16[384,2048]{1,0:T(8,128)(2,1)}, u32[]{:S(2)}, u32[]{:S(2)}) collective-permute-start(bf16[384,2048]{1,0:T(8,128)(2,1)S(1)} %collective-permute-done), channel_id=1, source_target_pairs={{0,1},{1,2},{2,3},{3,0},{4,5},{5,6},{6,7},{7,4},{8,9},{9,10},{10,1... | collective-permute-start | bytes 4718600 | tf_op jit(solution)/shard_map/ppermute | solution.py:13
  117.7 320.3 %reduce-scatter.2.cloned.1.call-start = ((), (), s32[]{:S(2)}) async-start(), calls=%async_computation.5 | async-start | bytes 7864320 | tf_op jit(solution)/shard_map/reduce_scatter | solution.py:65
  137.7 20.2 %collective-permute-start.2 = (bf16[384,2048]{1,0:T(8,128)(2,1)}, bf16[384,2048]{1,0:T(8,128)(2,1)}, u32[]{:S(2)}, u32[]{:S(2)}) collective-permute-start(bf16[384,2048]{1,0:T(8,128)(2,1)} %collective-permute-done.1), channel_id=1, source_target_pairs={{0,1},{1,2},{2,3},{3,0},{4,5},{5,6},{6,7},{7,4},{8,9},{9,10},{10,1... | collective-permute-start | bytes 4718600 | tf_op jit(solution)/shard_map/ppermute | solution.py:13
  195.0 79.0 %copy-start.4 = (f32[1376]{0:T(1024)S(1)}, f32[1376]{0:T(1024)}, u32[]{:S(2)}) copy-start(f32[1376]{0:T(1024)} %param.16) | copy-start | bytes 16516
  365.7 75.6 %copy-start.1 = (bf16[384,2048]{1,0:T(8,128)(2,1)S(1)}, bf16[384,2048]{1,0:T(8,128)(2,1)}, u32[]{:S(2)}) copy-start(bf16[384,2048]{1,0:T(8,128)(2,1)} %param.9) | copy-start | bytes 4718596
Sparse Core Ops, SparseCore 0:
  10.2 79.7 all-gather.4
  92.0 90.1 all-gather.6
  184.3 89.7 all-gather.8
  276.0 89.7 all-gather.10
  381.0 57.0 reduce-scatter.1
